TPU v7x, 32 devices: a whole 2x2x4 slice. The times are simulated.
32 devices in a mesh: ep: 16 (over z, y, x), tp: 2 (over core).
Axes of the slice: x: 2, y: 2, z: 4, core: 2. Of those that a mesh axis runs over, the one named last changes fastest.
Arguments:
- tokens: bfloat16 [4096, 2048], P(('ep', 'tp')), may hold values from -6 to 6
- norm_gain: float32 [2048], replicated, may hold values from 0.25 to 4
- routes: int32 [4096, 2], P(('ep', 'tp')), may hold values from 0 to 15, all different within a row; in each aligned block of 128 rows (0 to 127, 128 to 255, ...) at most 22 rows name the same one
- route_weights: float32 [4096, 2], P(('ep', 'tp')), may hold values from 0.1 to 1
- w_gate: bfloat16 [16, 2048, 1024], P('ep', None, 'tp'), may hold values from -0.125 to 0.125
- w_up: bfloat16 [16, 2048, 1024], P('ep', None, 'tp'), may hold values from -0.125 to 0.125
- w_down: bfloat16 [16, 1024, 2048], P('ep', 'tp'), may hold values from -0.1875 to 0.1875
- dense_in: bfloat16 [2048, 256], P('ep'), may hold values from -0.125 to 0.125
- dense_out: bfloat16 [2048, 256], P('ep'), may hold values from -0.375 to 0.375
- dense_gate: float32 [2048], replicated, may hold values from -6 to 6
Outputs:
- mixed: bfloat16 [4096, 2048], P(('ep', 'tp'))
Inputs may be any that keep to these rules, and one draw needn't show every extreme that they name: `routes`: each row names 2 different experts. Among the 128 rows of one device no expert is named more than 22 times; every draw has a device and an expert with exactly 22.
All inputs are finite; a program needn't handle non-finite values.
Results may differ from a plain program's by a relative error of at most 0.0074.
Values may be sent and summed in bfloat16 or wider, within the bound.
A program may use at most 128 MiB of HBM per device.

v0:
```python
import jax
import jax.numpy as jnp
from jax import lax
from jax.sharding import PartitionSpec as P

CLAMP_LIMIT = 7.0
SLOPE_ALPHA = 1.702
NORM_EPS = 1e-06


def rms_normed(tokens, norm_gain):
    widened = tokens.astype(jnp.float32)
    inv_scale = lax.rsqrt(jnp.mean(widened * widened, axis=1, keepdims=True) + NORM_EPS)
    return (widened * inv_scale * norm_gain).astype(jnp.bfloat16)


def clamped_unit(gate_pre, up_pre):
    gate_clip = jnp.minimum(gate_pre, CLAMP_LIMIT)
    up_clip = jnp.clip(up_pre, -CLAMP_LIMIT, CLAMP_LIMIT)
    return ((up_clip + 1.0) * gate_clip * jax.nn.sigmoid(SLOPE_ALPHA * gate_clip)).astype(
        jnp.bfloat16
    )


def rounded_term(hidden_rows, down_rows):
    partial_value = jnp.dot(hidden_rows, down_rows, preferred_element_type=jnp.float32).astype(
        jnp.bfloat16
    )
    return lax.optimization_barrier(partial_value).astype(jnp.float32)


def shards(
    tokens, norm_gain, routes, route_weights, w_gate, w_up, w_down, dense_in, dense_out, dense_gate
):
    tok_rows, model_width = tokens.shape
    top_count = routes.shape[1]
    sources = lax.axis_size("ep")
    experts = sources * w_gate.shape[0]
    core_count = lax.axis_size("tp")
    capacity = (4 * tok_rows * top_count + 3 * experts - 1) // (3 * experts)
    entries = tok_rows * top_count
    normed = rms_normed(tokens, norm_gain)
    flat_routes = routes.reshape(entries)
    onehot = flat_routes[:, None] == lax.broadcasted_iota(jnp.int32, (1, experts), 1)
    earlier_mask = (
        lax.broadcasted_iota(jnp.int32, (entries, entries), 0)
        > lax.broadcasted_iota(jnp.int32, (entries, entries), 1)
    ).astype(jnp.bfloat16)
    counted = jnp.dot(earlier_mask, onehot.astype(jnp.bfloat16), preferred_element_type=jnp.float32)
    slot_index = jnp.sum(jnp.where(onehot, counted, 0.0), axis=1).astype(jnp.int32)
    position = flat_routes * capacity + slot_index
    places = position[None, :] == lax.broadcasted_iota(jnp.int32, (experts * capacity, 1), 0)
    filled = jnp.any(places, axis=1)
    source_entry = jnp.sum(
        jnp.where(places, lax.broadcasted_iota(jnp.int32, (1, entries), 1), 0), axis=1
    )
    buffer = jnp.where(
        filled[:, None], normed[source_entry // top_count], jnp.zeros((), jnp.bfloat16)
    )
    buffer = buffer.reshape(experts, capacity, model_width)
    gate_w = w_gate[0]
    up_w = w_up[0]
    down_w = w_down[0]
    gate_w, up_w, down_w = (
        lax.all_gather(gate_w, "tp", axis=1, tiled=True),
        lax.all_gather(up_w, "tp", axis=1, tiled=True),
        lax.all_gather(down_w, "tp", axis=0, tiled=True),
    )
    received = lax.all_to_all(buffer, "ep", split_axis=0, concat_axis=0, tiled=True)
    slot_count = received.shape[1]
    flat_rows = received.reshape(sources * slot_count, model_width)
    hidden = clamped_unit(
        jnp.dot(flat_rows, gate_w, preferred_element_type=jnp.float32),
        jnp.dot(flat_rows, up_w, preferred_element_type=jnp.float32),
    )
    half_width = hidden.shape[1] // core_count
    summed = rounded_term(hidden[:, :half_width], down_w[:half_width])
    summed = summed + rounded_term(
        hidden[:, half_width : half_width + half_width],
        down_w[half_width : half_width + half_width],
    )
    expert_out = summed.astype(jnp.bfloat16).reshape(sources, slot_count, model_width)
    returned = lax.all_to_all(expert_out, "ep", split_axis=0, concat_axis=0, tiled=True)
    flat_returned = returned.reshape(experts * capacity, model_width)
    picked = flat_returned[position].astype(jnp.float32).reshape(tok_rows, top_count, model_width)
    weighted = jnp.sum(picked * route_weights[:, :, None], axis=1)
    whole_in, whole_out = (
        lax.all_gather(dense_in, "ep", axis=0, tiled=True),
        lax.all_gather(dense_out, "ep", axis=0, tiled=True),
    )
    dense_hidden = jax.nn.silu(
        jnp.dot(normed, whole_in, preferred_element_type=jnp.float32)
    ).astype(jnp.bfloat16)
    branch = lax.dot_general(
        dense_hidden, whole_out, (((1,), (1,)), ((), ())), preferred_element_type=jnp.float32
    )
    return (weighted + jax.nn.sigmoid(dense_gate) * branch).astype(jnp.bfloat16)


def solution(mesh):
    placed = (
        P(("ep", "tp"), None),
        P(),
        P(("ep", "tp"), None),
        P(("ep", "tp"), None),
        P("ep", None, "tp"),
        P("ep", None, "tp"),
        P("ep", "tp", None),
        P("ep", None),
        P("ep", None),
        P(),
    )
    return jax.shard_map(
        shards, mesh=mesh, in_specs=placed, out_specs=P(("ep", "tp"), None), check_vma=False
    )
```

profile of v0, /device:TPU:0, one launch (start us, length us, event | category | flops | bytes accessed | tf_op | source)
XLA Modules:
  0.0 191.8 jit_solution(7920561846483275655)
XLA Ops:
  6.5 0.0 all-gather.15.cloned.1.call-start
  6.5 0.7 all-gather.15.cloned.1.call-update
  7.3 0.0 all-gather.13.cloned.1.call-start
  7.3 0.7 all-gather.13.cloned.1.call-update
  8.0 0.0 copy-start.4
  8.0 0.0 copy-start
  8.0 0.0 copy-start.2
  8.0 0.0 all-gather.17.cloned.1.call-start
  8.1 0.7 all-gather.17.cloned.1.call-update
  8.8 0.0 copy-done.4
  8.8 0.1 copy.15
  8.9 0.1 reshape.135
  9.0 0.2 fusion.14
  9.3 0.1 select_reduce_fusion
  9.4 0.0 copy-done
  9.5 0.2 fusion.15
  9.7 0.0 copy-done.2
  9.7 0.2 fusion.17
  9.9 2.5 %gather_fusion = bf16[352,2048]{1,0:T(8,128)(2,1)S(1)} fusion(bf16[128,2048]{1,0:T(8,128)(2,1)S(1)} %fusion.17, s32[1024]{0:T(1024)S(1)} %pad_clamp_fusion.1), kind=kCustom, calls=%fused_computation | custom fusion | bytes 2884992 | tf_op jit(solution)/shard_map/gather | solution.py:58
  12.3 0.4 gather.9
  12.8 0.2 fusion.20
  12.9 0.1 broadcast_in_dim.39
  13.0 1.4 broadcast_select_fusion
  14.4 8.3 %all-to-all-start = ((bf16[16,22,2048]{2,1,0:T(8,128)(2,1)}), bf16[16,22,2048]{2,1,0:T(8,128)(2,1)S(1)}, u32[]{:S(2)}, u32[]{:S(2)}) async-start(bf16[16,22,2048]{2,1,0:T(8,128)(2,1)} %broadcast_select_fusion), calls=%async_computation | async-start | bytes 3145728 | tf_op jit(solution)/shard_map/all_to_all | solution.py:69
  22.7 0.0 all-gather.11.cloned.1.call-start
  22.8 0.5 all-gather.11.cloned.1.call-update
  23.3 33.5 %all-to-all-done = bf16[16,22,2048]{2,1,0:T(8,128)(2,1)S(1)} async-done(((bf16[16,22,2048]{2,1,0:T(8,128)(2,1)}), bf16[16,22,2048]{2,1,0:T(8,128)(2,1)S(1)}, u32[]{:S(2)}, u32[]{:S(2)}) %all-to-all-start) | async-done | bytes 1441824 | tf_op jit(solution)/shard_map/all_to_all | solution.py:69
  56.8 0.4 reshape.136
  57.3 0.0 all-gather.15.cloned.1.call-done
  57.3 5.0 %fusion.9 = f32[352,1024]{1,0:T(8,128)} fusion(bf16[352,2048]{1,0:T(8,128)(2,1)S(1)} %reshape.136, bf16[1,2048,1024]{2,1,0:T(8,128)(2,1)} %all-gather.15.cloned.1.call-done), kind=kOutput, calls=%fused_computation.17 | convolution fusion | flops 1476755456 | bytes 7077888 | tf_op jit(solution)/shard_map/dot_general | solution.py:73
  62.3 0.0 all-gather.13.cloned.1.call-done
  62.3 4.5 %multiply_convert_fusion = bf16[352,1024]{1,0:T(8,128)(2,1)S(1)} fusion(f32[352,1024]{1,0:T(8,128)} %fusion.9, bf16[352,2048]{1,0:T(8,128)(2,1)S(1)} %reshape.136, bf16[1,2048,1024]{2,1,0:T(8,128)(2,1)} %all-gather.13.cloned.1.call-done), kind=kOutput, calls=%fused_computation.18 | convolution fusion | flops 1479639040 | bytes 7798784 | tf_op jit(solution)/shard_map/dot_general | solution.py:74
  66.8 0.0 all-gather.17.cloned.1.call-done
  66.8 0.0 copy-start.6
  66.8 2.7 %convolution_convert_fusion.1 = bf16[352,2048]{1,0:T(8,128)(2,1)S(1)} fusion(bf16[1,1024,2048]{2,1,0:T(8,128)(2,1)} %all-gather.17.cloned.1.call-done, bf16[352,1024]{1,0:T(8,128)(2,1)S(1)} %multiply_convert_fusion), kind=kOutput, calls=%fused_computation.8 | convolution fusion | flops 738918400 | bytes 3899392 | tf_op jit(solution)/shard_map/dot_general | solution.py:26
  69.5 0.2 copy-done.6
  69.6 0.9 convolution_convert_fusion
  70.6 0.5 add_convert_fusion
  71.1 1.4 reshape.137
  72.5 0.0 copy-start.5
  72.5 0.0 copy-start.3
  72.5 7.9 %all-to-all-start.1 = ((bf16[16,22,2048]{2,1,0:T(8,128)(2,1)}), bf16[16,22,2048]{2,1,0:T(8,128)(2,1)S(1)}, u32[]{:S(2)}, u32[]{:S(2)}) async-start(bf16[16,22,2048]{2,1,0:T(8,128)(2,1)} %reshape.137), calls=%async_computation.1 | async-start | bytes 3145728 | tf_op jit(solution)/shard_map/all_to_all | solution.py:83
  80.4 0.2 all-gather.9.cloned.1.call-start
  80.6 0.4 all-gather.9.cloned.1.call-update
  81.0 0.1 copy.16
  81.1 0.1 mul.88
  81.2 0.0 copy-done.5
  81.3 0.7 copy.17
  82.0 0.0 copy-done.3
  82.0 38.2 %all-to-all-done.1 = bf16[16,22,2048]{2,1,0:T(8,128)(2,1)S(1)} async-done(((bf16[16,22,2048]{2,1,0:T(8,128)(2,1)}), bf16[16,22,2048]{2,1,0:T(8,128)(2,1)S(1)}, u32[]{:S(2)}, u32[]{:S(2)}) %all-to-all-start.1) | async-done | bytes 1441824 | tf_op jit(solution)/shard_map/all_to_all | solution.py:83
  120.2 0.4 reshape.138
  120.6 2.3 %gather_fusion.1 = bf16[256,2048]{1,0:T(8,128)(2,1)} fusion(bf16[352,2048]{1,0:T(8,128)(2,1)S(1)} %reshape.138, s32[1024]{0:T(1024)S(1)} %pad_clamp_fusion), kind=kCustom, calls=%fused_computation.1 | custom fusion | bytes 2098176 | tf_op jit(solution)/shard_map/gather | solution.py:85
  123.0 0.0 copy-start.1
  123.0 2.4 %reshape.139 = f32[128,2,2048]{2,1,0:T(2,128)S(1)} reshape(bf16[256,2048]{1,0:T(8,128)(2,1)} %gather_fusion.1) | data formatting | bytes 3145728 | tf_op jit(solution)/shard_map/convert_element_type | solution.py:85
  125.4 0.0 copy-done.1
  125.4 4.1 %multiply_reduce_fusion = f32[128,2048]{1,0:T(8,128)} fusion(f32[128,2,2048]{2,1,0:T(2,128)S(1)} %reshape.139, f32[128,2]{1,0:T(8,128)S(1)} %copy-done.1), kind=kLoop, calls=%fused_computation.14 | loop fusion | flops 786432 | bytes 3146752 | tf_op jit(solution)/shard_map/reduce_sum | solution.py:86
  129.4 0.0 all-gather.11.cloned.1.call-done
  129.4 52.3 %all-gather.9.cloned.1.call-done = bf16[2048,256]{1,0:T(8,128)(2,1)} async-done(((bf16[128,256]{1,0:T(8,128)(2,1)}), bf16[2048,256]{1,0:T(8,128)(2,1)}) %all-gather.9.cloned.1.call-update) | async-done | bytes 1048592 | tf_op jit(solution)/shard_map/all_gather | solution.py:88
  181.7 3.6 %fusion.5 = bf16[128,2048]{1,0:T(8,128)(2,1)} fusion(f32[128,2048]{1,0:T(8,128)} %multiply_reduce_fusion, bf16[2048,256]{1,0:T(8,128)(2,1)} %all-gather.11.cloned.1.call-done, f32[2048]{0:T(1024)S(1)} %add_divide_fusion, bf16[128,2048]{1,0:T(8,128)(2,1)S(1)} %fusion.17, bf16[2048,256]{1,0:T(8,128)(2,1)} %all-gather.9.cloned.1.call-done), kind=kOutput, calls=%fused_computation.11 | convolution fusion | flops 269385728 | bytes 4202496 | tf_op jit(solution)/shard_map/dot_general | solution.py:94
  (9 shorter events, 0.1 us)
Async XLA Ops:
  6.5 50.8 %all-gather.15.cloned.1.call-start = ((), (), s32[]{:S(2)}) async-start(), calls=%async_computation.5 | async-start | bytes 6291456 | tf_op jit(solution)/shard_map/all_gather | solution.py:65
  7.3 55.0 %all-gather.13.cloned.1.call-start = ((), (), s32[]{:S(2)}) async-start(), calls=%async_computation.4 | async-start | bytes 6291456 | tf_op jit(solution)/shard_map/all_gather | solution.py:66
  8.0 0.8 copy-start.4
  8.0 1.4 copy-start
  8.0 1.6 copy-start.2
  8.0 58.8 %all-gather.17.cloned.1.call-start = ((), (), s32[]{:S(2)}) async-start(), calls=%async_computation.6 | async-start | bytes 6291456 | tf_op jit(solution)/shard_map/all_gather | solution.py:67
  14.4 42.4 %all-to-all-start = ((bf16[16,22,2048]{2,1,0:T(8,128)(2,1)}), bf16[16,22,2048]{2,1,0:T(8,128)(2,1)S(1)}, u32[]{:S(2)}, u32[]{:S(2)}) async-start(bf16[16,22,2048]{2,1,0:T(8,128)(2,1)} %broadcast_select_fusion), calls=%async_computation | async-start | bytes 3145728 | tf_op jit(solution)/shard_map/all_to_all | solution.py:69
  22.7 106.7 %all-gather.11.cloned.1.call-start = ((), (), s32[]{:S(2)}) async-start(), calls=%async_computation.3 | async-start | bytes 1114112 | tf_op jit(solution)/shard_map/all_gather | solution.py:89
  66.8 2.8 %copy-start.6 = (bf16[1,1024,2048]{2,1,0:T(8,128)(2,1)S(1)}, bf16[1,1024,2048]{2,1,0:T(8,128)(2,1)}, u32[]{:S(2)}) copy-start(bf16[1,1024,2048]{2,1,0:T(8,128)(2,1)} %all-gather.17.cloned.1.call-done) | copy-start | bytes 12582916
  72.5 8.8 %copy-start.5 = (f32[128,2]{0,1:T(2,128)S(1)}, f32[128,2]{0,1:T(2,128)}, u32[]{:S(2)}) copy-start(f32[128,2]{0,1:T(2,128)} %param.13) | copy-start | bytes 3076
  72.5 9.5 %copy-start.3 = (f32[2048]{0:T(1024)S(1)}, f32[2048]{0:T(1024)}, u32[]{:S(2)}) copy-start(f32[2048]{0:T(1024)} %param.19) | copy-start | bytes 24580
  72.5 47.7 %all-to-all-start.1 = ((bf16[16,22,2048]{2,1,0:T(8,128)(2,1)}), bf16[16,22,2048]{2,1,0:T(8,128)(2,1)S(1)}, u32[]{:S(2)}, u32[]{:S(2)}) async-start(bf16[16,22,2048]{2,1,0:T(8,128)(2,1)} %reshape.137), calls=%async_computation.1 | async-start | bytes 3145728 | tf_op jit(solution)/shard_map/all_to_all | solution.py:83
  80.4 101.3 %all-gather.9.cloned.1.call-start = ((), (), s32[]{:S(2)}) async-start(), calls=%async_computation.2 | async-start | bytes 1114112 | tf_op jit(solution)/shard_map/all_gather | solution.py:88
  123.0 2.4 %copy-start.1 = (f32[128,2]{1,0:T(8,128)S(1)}, f32[128,2]{1,0:T(8,128)}, u32[]{:S(2)}) copy-start(f32[128,2]{1,0:T(8,128)} %copy.17) | copy-start | bytes 3076
Sparse Core Ops, SparseCore 0:
  8.9 16.3 all-gather.14
  26.8 14.8 all-gather.12
  43.3 14.8 all-gather.16
  60.8 63.4 all-gather.10
  126.8 54.8 all-gather.8
where the time goes:
time: 192 us
  waiting for transfers between devices  127 us (66%)
  matrix products  16.8 us (9%)
  starting transfers between devices  16.6 us (9%)
  between operations  13.4 us (7%)
  local copies, waits for them, and re-layouts  11.4 us (6%)
  other arithmetic  6.7 us (3%)
    all_gather x1, waiting for transfers between devices, shards(): lax.all_gather(dense_in, 'ep', axis=0, tiled=True)  52.3 us
    all_to_all x1, waiting for transfers between devices, shards(): lax.all_to_all(expert_out, 'ep', split_axis=0, concat_axis=0, tiled=True)  38.2 us
    all_to_all x1, waiting for transfers between devices, shards(): lax.all_to_all(buffer, 'ep', split_axis=0, concat_axis=0, tiled=True)  33.5 us
    all_to_all x1, starting transfers between devices, shards(): lax.all_to_all(buffer, 'ep', split_axis=0, concat_axis=0, tiled=True)  8.34 us
    all_to_all x1, starting transfers between devices, shards(): lax.all_to_all(expert_out, 'ep', split_axis=0, concat_axis=0, tiled=True)  7.9 us
    dot_general x1, matrix products, shards(): jnp.dot(flat_rows, gate_w, preferred_element_type=jnp.float32)  5 us
    dot_general x1, matrix products, shards(): jnp.dot(flat_rows, up_w, preferred_element_type=jnp.float32)  4.48 us
    reduce_sum x1, other arithmetic, shards(): weighted = jnp.sum(picked * route_weights[:, :, None], axis=1)  4.05 us
  transfers between devices with their start and end apart: 7, of which 3 were waited for; matrix products, arithmetic and copies ran while one was open for 16% of the time, Pallas kernels for 0%

commit v1 on v0

v1 whole, which is shorter than its diff:
```python
import functools

import jax
import jax.numpy as jnp
from jax import lax
from jax.experimental import pallas as pl
from jax.experimental.pallas import tpu as pltpu
from jax.sharding import PartitionSpec as P

CLAMP_LIMIT = 7.0
SLOPE_ALPHA = 1.702
NORM_EPS = 1e-06
MESH = pl.DeviceIdType.MESH
F32 = jnp.float32
BF16 = jnp.bfloat16


def clamped_unit(gate_pre, up_pre):
    gate_clip = jnp.minimum(gate_pre, CLAMP_LIMIT)
    up_clip = jnp.clip(up_pre, -CLAMP_LIMIT, CLAMP_LIMIT)
    return ((up_clip + 1.0) * gate_clip * jax.nn.sigmoid(SLOPE_ALPHA * gate_clip)).astype(BF16)


def layer_kernel(
    sizes,
    routes_ref,
    weights_ref,
    tokens_ref,
    gain_ref,
    dgate_ref,
    din_ref,
    dout_ref,
    wg_ref,
    wu_ref,
    wd_ref,
    out_ref,
    normed,
    slots,
    buf,
    recv,
    outb,
    ret,
    wgs,
    wus,
    wds,
    hid,
    dn,
    acc,
    send1,
    recv1,
    send2,
    recv2,
    w_local,
    w_send,
    w_recv,
    ds1,
    dr1,
    ds2,
    dr2,
    ds3,
    dr3,
):
    n, n1, n2, cap = sizes
    rows, width = tokens_ref.shape
    half = wg_ref.shape[1]
    me = lax.axis_index("ep")
    core = lax.axis_index("tp")
    plane, spot = me // n2, me % n2
    peer = 1 - core

    barrier = pltpu.get_barrier_semaphore()

    def greet(i, carry):
        pl.semaphore_signal(
            barrier, inc=1, device_id={"ep": (me + i) % n}, device_id_type=MESH
        )
        return carry

    lax.fori_loop(1, n, greet, 0)
    pl.semaphore_signal(barrier, inc=1, device_id={"tp": peer}, device_id_type=MESH)

    weight_pairs = ((wg_ref, wgs), (wu_ref, wus), (wd_ref, wds))
    for i, (src, dst) in enumerate(weight_pairs):
        pltpu.make_async_copy(src, dst.at[0], w_local.at[i]).start()

    @pl.when(core == 0)
    def _():
        dn[0, plane, spot] = din_ref[...]

    @pl.when(core == 1)
    def _():
        dn[1, plane, spot] = dout_ref[...]

    widened = tokens_ref[...].astype(F32)
    inv_scale = lax.rsqrt(jnp.mean(widened * widened, axis=1, keepdims=True) + NORM_EPS)
    normed[...] = (widened * inv_scale * gain_ref[...]).astype(BF16)

    expert_ids = lax.broadcasted_iota(jnp.int32, (n, rows), 0)
    chosen = (routes_ref[0:1, :] == expert_ids) | (routes_ref[1:2, :] == expert_ids)
    earlier = (
        lax.broadcasted_iota(jnp.int32, (rows, rows), 0)
        < lax.broadcasted_iota(jnp.int32, (rows, rows), 1)
    )
    counted = jnp.dot(
        jnp.where(chosen, 1.0, 0.0).astype(BF16),
        jnp.where(earlier, 1.0, 0.0).astype(BF16),
        preferred_element_type=F32,
    )
    slots[...] = jnp.where(chosen, counted.astype(jnp.int32), -1)

    pl.semaphore_wait(barrier, n)

    def weight_copy(i):
        src, dst = weight_pairs[i]
        return pltpu.make_async_remote_copy(
            src_ref=src,
            dst_ref=dst.at[1],
            send_sem=w_send.at[i],
            recv_sem=w_recv.at[i],
            device_id={"tp": peer},
            device_id_type=MESH,
        )

    def dense_copy1(other):
        return pltpu.make_async_remote_copy(
            src_ref=dn.at[core, plane, spot],
            dst_ref=dn.at[core, plane, spot],
            send_sem=ds1.at[other],
            recv_sem=dr1.at[plane],
            device_id={"ep": other * n2 + spot},
            device_id_type=MESH,
        )

    def dense_wait1(other):
        pltpu.make_async_remote_copy(
            src_ref=dn.at[core, other, spot],
            dst_ref=dn.at[core, other, spot],
            send_sem=ds1.at[other],
            recv_sem=dr1.at[other],
            device_id={"ep": other * n2 + spot},
            device_id_type=MESH,
        ).wait_recv()

    def dense_copy2(other, slot):
        return pltpu.make_async_remote_copy(
            src_ref=dn.at[core, :, slot],
            dst_ref=dn.at[core, :, slot],
            send_sem=ds2.at[other],
            recv_sem=dr2.at[slot],
            device_id={"ep": plane * n2 + other},
            device_id_type=MESH,
        )

    def dense_copy3(which):
        return pltpu.make_async_remote_copy(
            src_ref=dn.at[which],
            dst_ref=dn.at[which],
            send_sem=ds3,
            recv_sem=dr3,
            device_id={"tp": peer},
            device_id_type=MESH,
        )

    def each(count, act):
        def step(i, carry):
            act(i)
            return carry

        lax.fori_loop(0, count, step, 0)

    each(n1 - 1, lambda i: dense_copy1((plane + 1 + i) % n1).start())
    for i in range(3):
        weight_copy(i).start()

    def dispatch(dst, slot):
        return pltpu.make_async_remote_copy(
            src_ref=buf.at[dst],
            dst_ref=recv.at[slot],
            send_sem=send1.at[dst],
            recv_sem=recv1.at[slot],
            device_id={"ep": dst},
            device_id_type=MESH,
        )

    def give_back(dst, slot):
        return pltpu.make_async_remote_copy(
            src_ref=outb.at[dst],
            dst_ref=ret.at[slot],
            send_sem=send2.at[dst],
            recv_sem=recv2.at[slot],
            device_id={"ep": dst},
            device_id_type=MESH,
        )

    def shift_of(i):
        later = (n1 // 2 + i - 2) % (n1 - 1) + 1
        return jnp.where(i == 0, 0, later)

    tile = min(512, width)

    def send_group(i):
        group = (plane + shift_of((i + 1) % n1)) % n1
        first = group * n2
        wanted = slots[pl.ds(first, n2), :]
        picks = wanted[:, None, :] == lax.broadcasted_iota(jnp.int32, (n2, cap, rows), 1)
        picks = jnp.where(picks, 1.0, 0.0).reshape(n2 * cap, rows).astype(BF16)
        for low in range(0, width, tile):
            found = jnp.dot(picks, normed[:, low : low + tile], preferred_element_type=F32)
            buf[pl.ds(first, n2), :, low : low + tile] = found.reshape(n2, cap, tile).astype(BF16)

        def start(j):
            dst = first + (spot + 1 + j) % n2

            @pl.when(dst != me)
            def _():
                dispatch(dst, me).start()

            @pl.when(dst == me)
            def _():
                recv[me] = buf[me]

        each(n2, start)

    each(n1, send_group)

    each(n1 - 1, lambda i: dense_wait1((plane + 1 + i) % n1))
    each(n2 - 1, lambda i: dense_copy2((spot + 1 + i) % n2, spot).start())

    for i, (src, dst) in enumerate(weight_pairs):
        pltpu.make_async_copy(src, dst.at[0], w_local.at[i]).wait()
    for i in range(3):
        weight_copy(i).wait()

    piece = min(256, half)

    def run_group(i):
        group = (plane - shift_of(i) + n1) % n1
        first = group * n2

        def arrive(j):
            src = first + j

            @pl.when(src != me)
            def _():
                dispatch(src, src).wait_recv()

        each(n2, arrive)
        x = recv[pl.ds(first, n2)].astype(F32).reshape(n2 * cap, width).astype(BF16)
        for part in range(2):
            for low in range(0, half, piece):
                gate_pre = jnp.dot(
                    x, wgs[part, :, low : low + piece], preferred_element_type=F32
                )
                up_pre = jnp.dot(x, wus[part, :, low : low + piece], preferred_element_type=F32)
                hid[part, :, low : low + piece] = clamped_unit(gate_pre, up_pre)
        for low in range(0, width, tile):
            total = jnp.zeros((n2 * cap, tile), F32)
            for part in range(2):
                partial = jnp.dot(
                    hid[part], wds[part, :, low : low + tile], preferred_element_type=F32
                )
                total = total + partial.astype(BF16).astype(F32)
            outb[pl.ds(first, n2), :, low : low + tile] = total.reshape(n2, cap, tile).astype(BF16)

        def start(j):
            dst = first + (spot + 1 + j) % n2

            @pl.when(dst != me)
            def _():
                give_back(dst, me).start()

            @pl.when(dst == me)
            def _():
                ret[me] = outb[me]

        each(n2, start)

    each(n1 // 2, run_group)
    each(n2 - 1, lambda i: dense_copy2((spot + 1 + i) % n2, (spot + 1 + i) % n2).wait_recv())
    dense_copy3(core).start()
    each(n1 - n1 // 2, lambda i: run_group(i + n1 // 2))

    dense_copy3(core).wait_send()
    dense_copy3(peer).wait_recv()
    depth = din_ref.shape[1]
    dense_pre = jnp.dot(
        normed[...], dn[0].reshape(width, depth), preferred_element_type=F32
    )
    dense_hidden = jax.nn.silu(dense_pre).astype(BF16)
    step = width // n1
    for z in range(n1):
        branch = lax.dot_general(
            dense_hidden,
            dn[1, z].reshape(step, depth),
            (((1,), (1,)), ((), ())),
            preferred_element_type=F32,
        )
        acc[:, z * step : (z + 1) * step] = (
            jax.nn.sigmoid(dgate_ref[:, z * step : (z + 1) * step]) * branch
        )

    def settle(i):
        other = (me + 1 + i) % n
        give_back(other, other).wait_recv()

    each(n - 1, settle)

    places = lax.broadcasted_iota(jnp.int32, (n, cap, rows), 1)
    here = slots[...][:, None, :] == places
    takes = []
    for k in range(2):
        mine = (routes_ref[k : k + 1, :] == expert_ids)[:, None, :]
        take = jnp.where(here & mine, 1.0, 0.0).reshape(n * cap, rows)
        takes.append(take.T.astype(BF16))
    for low in range(0, width, tile):
        back = ret[:, :, low : low + tile].astype(F32).reshape(n * cap, tile).astype(BF16)
        total = acc[:, low : low + tile]
        for k in range(2):
            picked = jnp.dot(takes[k], back, preferred_element_type=F32)
            total = total + picked * weights_ref[:, k : k + 1]
        out_ref[:, low : low + tile] = total.astype(BF16)

    def drain(i):
        other = (me + 1 + i) % n
        dispatch(other, me).wait_send()
        give_back(other, me).wait_send()

    each(n - 1, drain)
    each(n1 - 1, lambda i: dense_copy1((plane + 1 + i) % n1).wait_send())
    each(n2 - 1, lambda i: dense_copy2((spot + 1 + i) % n2, spot).wait_send())


def shards(
    tokens, norm_gain, routes, route_weights, w_gate, w_up, w_down, dense_in, dense_out, dense_gate
):
    rows, width = tokens.shape
    top_count = routes.shape[1]
    n = lax.axis_size("ep")
    capacity = (4 * rows * top_count + 3 * n - 1) // (3 * n)
    cap = -(-capacity // 8) * 8
    n2 = 1
    while n2 * n2 < n:
        n2 *= 2
    n1 = n // n2
    half = w_gate.shape[2]
    depth = dense_in.shape[1]
    vmem = pl.BlockSpec(memory_space=pltpu.VMEM)
    anywhere = pl.BlockSpec(memory_space=pl.ANY)
    dma = pltpu.SemaphoreType.DMA
    slab = pltpu.VMEM((n, cap, width), BF16)
    return pl.pallas_call(
        functools.partial(layer_kernel, (n, n1, n2, cap)),
        out_shape=jax.ShapeDtypeStruct((rows, width), BF16),
        in_specs=[vmem] * 7 + [anywhere] * 3,
        out_specs=vmem,
        scratch_shapes=[
            pltpu.VMEM((rows, width), BF16),
            pltpu.VMEM((n, rows), jnp.int32),
            slab,
            slab,
            slab,
            slab,
            pltpu.VMEM((2, width, half), BF16),
            pltpu.VMEM((2, width, half), BF16),
            pltpu.VMEM((2, half, width), BF16),
            pltpu.VMEM((2, n2 * cap, half), BF16),
            pltpu.VMEM((2, n1, n2, width // n, depth), BF16),
            pltpu.VMEM((rows, width), F32),
            dma((n,)),
            dma((n,)),
            dma((n,)),
            dma((n,)),
            dma((3,)),
            dma((3,)),
            dma((3,)),
            dma((n1,)),
            dma((n1,)),
            dma((n2,)),
            dma((n2,)),
            dma,
            dma,
        ],
        compiler_params=pltpu.CompilerParams(
            collective_id=0, has_side_effects=True, vmem_limit_bytes=60 * 1024 * 1024
        ),
    )(
        routes.T,
        route_weights,
        tokens,
        norm_gain.reshape(1, width),
        dense_gate.reshape(1, width),
        dense_in,
        dense_out,
        w_gate[0],
        w_up[0],
        w_down[0],
    )


def solution(mesh):
    placed = (
        P(("ep", "tp"), None),
        P(),
        P(("ep", "tp"), None),
        P(("ep", "tp"), None),
        P("ep", None, "tp"),
        P("ep", None, "tp"),
        P("ep", "tp", None),
        P("ep", None),
        P("ep", None),
        P(),
    )
    return jax.shard_map(
        shards, mesh=mesh, in_specs=placed, out_specs=P(("ep", "tp"), None), check_vma=False
    )
```

time: 192 us -> 89.7 us (0.47)
  waiting for transfers between devices: 127 us -> 0 us
  Pallas kernels: 0 us -> 86.2 us
  matrix products: 16.8 us -> 0 us
  starting transfers between devices: 16.6 us -> 0 us
  between operations: 13.4 us -> 0.01 us
  local copies, waits for them, and re-layouts: 11.4 us -> 3.29 us
  other arithmetic: 6.7 us -> 0 us
    pallas_call x0 -> x1, Pallas kernels: none -> 86.2 us  [shards(): pl.pallas_call(functools.partial(layer_kernel, (n, n1, n2, cap)), out_sha...]
    all_to_all x2 -> x0, waiting for transfers between devices: 71.7 us -> none  [the longest x1 38.2 us: shards(): lax.all_to_all(expert_out, 'ep', split_axis=0, concat_axis=0, tiled=True)]
    all_gather x5 -> x0, waiting for transfers between devices: 52.3 us -> none  [the longest x1 52.3 us: shards(): lax.all_gather(dense_in, 'ep', axis=0, tiled=True)]
    dot_general x6 -> x0, matrix products: 16.8 us -> none  [the longest x1 5 us: shards(): jnp.dot(flat_rows, gate_w, preferred_element_type=jnp.float32)]
    all_to_all x2 -> x0, starting transfers between devices: 16.2 us -> none  [the longest x1 8.34 us: shards(): lax.all_to_all(buffer, 'ep', split_axis=0, concat_axis=0, tiled=True)]
    gather x3 -> x0, local copies, waits for them, and re-layouts: 5.23 us -> none  [the longest x2 2.9 us: shards(): normed[source_entry // top_count]]
    reduce_sum x3 -> x0, other arithmetic: 4.39 us -> none  [the longest x1 4.05 us: shards(): weighted = jnp.sum(picked * route_weights[:, :, None], axis=1)]
    unnamed x5 -> x0, waiting for transfers between devices: 2.96 us -> none
  transfers between devices with their start and end apart: 7 -> 0, of which waited for: 3 -> 0; matrix products, arithmetic and copies ran while one was open for 16% -> 0% of each run, Pallas kernels for 0% -> 0%
where the time goes in v1:
time: 89.7 us; the launch traced here: 89.5 us
  Pallas kernels  86.2 us (96%)
  local copies, waits for them, and re-layouts  3.29 us (4%)
    pallas_call x1, Pallas kernels, shards(): pl.pallas_call(functools.partial(layer_kernel, (n, n1, n2, cap)), out_sha...  86.2 us
    unnamed x2, local copies, waits for them, and re-layouts  3.29 us

profile of v1, /device:TPU:0, one launch (start us, length us, event | category | flops | bytes accessed | tf_op | source)
XLA Modules:
  0.0 89.5 jit_solution(4722665947690900839)
XLA Ops:
  0.0 1.4 %copy.11.weights_ref = f32[128,2]{1,0:T(8,128)} copy(f32[128,2]{0,1:T(2,128)} %param.13) | data formatting | bytes 2048 | tf_op args[3]
  1.4 86.2 %shard_map.100 = bf16[128,2048]{1,0:T(8,128)(2,1)} custom-call(s32[2,128]{1,0:T(2,128)} %bitcast.11, f32[128,2]{1,0:T(8,128)} %copy.11.weights_ref, bf16[128,2048]{1,0:T(8,128)(2,1)} %tokens_ref.1, f32[1,2048]{1,0:T(1,128)} %bitcast.9, f32[1,2048]{1,0:T(1,128)} %bitcast.10, bf16[128,256]{1,0:T(8,128)(2,1)} %din_ref.1, bf16[128,256]{1,0:T(8,128)(2,1)} %dout_ref.1, ...), custom_call_target="tpu_custom_call" | custom-call | tf_op jit(solution)/shard_map/pallas_call | solution.py:351
  87.6 1.9 %copy.13 = bf16[128,2048]{1,0:T(8,128)(2,1)} copy(bf16[128,2048]{1,0:T(8,128)(2,1)} %shard_map.100) | data formatting | bytes 1048576

commit v2 on v1

--- a/solution.py
+++ b/solution.py
@@ -1,4 +1,5 @@
 import functools
+import math
 
 import jax
 import jax.numpy as jnp
@@ -23,6 +24,7 @@
 
 def layer_kernel(
     sizes,
+    routes_t_ref,
     routes_ref,
     weights_ref,
     tokens_ref,
@@ -35,7 +37,13 @@
     wd_ref,
     out_ref,
     normed,
-    slots,
+    keys,
+    stacked,
+    places,
+    xs,
+    totals,
+    unpack_ref,
+    pack_ref,
     buf,
     recv,
     outb,
@@ -60,9 +68,11 @@
     ds3,
     dr3,
 ):
-    n, n1, n2, cap = sizes
+    n, n1, n2, cap, blocks = sizes
     rows, width = tokens_ref.shape
     half = wg_ref.shape[1]
+    tall, tile = blocks * cap, width // blocks
+    group_rows, packed_rows = n2 * cap, n2 * blocks * cap
     me = lax.axis_index("ep")
     core = lax.axis_index("tp")
     plane, spot = me // n2, me % n2
@@ -94,9 +104,11 @@
     widened = tokens_ref[...].astype(F32)
     inv_scale = lax.rsqrt(jnp.mean(widened * widened, axis=1, keepdims=True) + NORM_EPS)
     normed[...] = (widened * inv_scale * gain_ref[...]).astype(BF16)
+    for j in range(blocks):
+        stacked[j * rows : (j + 1) * rows, :] = normed[:, j * tile : (j + 1) * tile]
 
     expert_ids = lax.broadcasted_iota(jnp.int32, (n, rows), 0)
-    chosen = (routes_ref[0:1, :] == expert_ids) | (routes_ref[1:2, :] == expert_ids)
+    chosen = (routes_t_ref[0:1, :] == expert_ids) | (routes_t_ref[1:2, :] == expert_ids)
     earlier = (
         lax.broadcasted_iota(jnp.int32, (rows, rows), 0)
         < lax.broadcasted_iota(jnp.int32, (rows, rows), 1)
@@ -106,7 +118,24 @@
         jnp.where(earlier, 1.0, 0.0).astype(BF16),
         preferred_element_type=F32,
     )
-    slots[...] = jnp.where(chosen, counted.astype(jnp.int32), -1)
+    for j in range(blocks):
+        found = jnp.where(chosen, counted.astype(jnp.int32) + j * cap, -1)
+        for z in range(n1):
+            keys[z, :, j * rows : (j + 1) * rows] = found[z * n2 : (z + 1) * n2]
+    experts_across = lax.broadcasted_iota(jnp.int32, (rows, n), 1)
+    takes = [routes_ref[:, k : k + 1] == experts_across for k in range(2)]
+    before = (
+        lax.broadcasted_iota(jnp.int32, (rows, rows), 0)
+        > lax.broadcasted_iota(jnp.int32, (rows, rows), 1)
+    )
+    counts = jnp.dot(
+        jnp.where(before, 1.0, 0.0).astype(BF16),
+        jnp.where(takes[0] | takes[1], 1.0, 0.0).astype(BF16),
+        preferred_element_type=F32,
+    )
+    for k in range(2):
+        slot = jnp.sum(jnp.where(takes[k], counts, 0.0), axis=1, keepdims=True)
+        places[:, k : k + 1] = routes_ref[:, k : k + 1] * tall + slot.astype(jnp.int32)
 
     pl.semaphore_wait(barrier, n)
 
@@ -121,25 +150,31 @@
             device_id_type=MESH,
         )
 
-    def dense_copy1(other):
-        return pltpu.make_async_remote_copy(
-            src_ref=dn.at[core, plane, spot],
-            dst_ref=dn.at[core, plane, spot],
-            send_sem=ds1.at[other],
-            recv_sem=dr1.at[plane],
+    def dense_copy1(bit, block):
+        other = plane + bit - 2 * bit * ((plane // bit) % 2)
+        return pltpu.make_async_remote_copy(
+            src_ref=dn.at[core, block, spot],
+            dst_ref=dn.at[core, block, spot],
+            send_sem=ds1.at[block],
+            recv_sem=dr1.at[block],
             device_id={"ep": other * n2 + spot},
             device_id_type=MESH,
         )
 
-    def dense_wait1(other):
-        pltpu.make_async_remote_copy(
-            src_ref=dn.at[core, other, spot],
-            dst_ref=dn.at[core, other, spot],
-            send_sem=ds1.at[other],
-            recv_sem=dr1.at[other],
-            device_id={"ep": other * n2 + spot},
-            device_id_type=MESH,
-        ).wait_recv()
+    bits = [1 << b for b in reversed(range(n1.bit_length() - 1))]
+
+    def dense_held(bit, where):
+        return [where % (2 * bit) + m * 2 * bit for m in range(n1 // (2 * bit))]
+
+    def dense_start(bit):
+        for block in dense_held(bit, plane):
+            dense_copy1(bit, block).start()
+
+    def dense_finish(bit):
+        for block in dense_held(bit, plane + bit - 2 * bit * ((plane // bit) % 2)):
+            dense_copy1(bit, block).wait_recv()
+        for block in dense_held(bit, plane):
+            dense_copy1(bit, block).wait_send()
 
     def dense_copy2(other, slot):
         return pltpu.make_async_remote_copy(
@@ -168,7 +203,7 @@
 
         lax.fori_loop(0, count, step, 0)
 
-    each(n1 - 1, lambda i: dense_copy1((plane + 1 + i) % n1).start())
+    dense_start(bits[0])
     for i in range(3):
         weight_copy(i).start()
 
@@ -196,17 +231,16 @@
         later = (n1 // 2 + i - 2) % (n1 - 1) + 1
         return jnp.where(i == 0, 0, later)
 
-    tile = min(512, width)
-
     def send_group(i):
         group = (plane + shift_of((i + 1) % n1)) % n1
         first = group * n2
-        wanted = slots[pl.ds(first, n2), :]
-        picks = wanted[:, None, :] == lax.broadcasted_iota(jnp.int32, (n2, cap, rows), 1)
-        picks = jnp.where(picks, 1.0, 0.0).reshape(n2 * cap, rows).astype(BF16)
-        for low in range(0, width, tile):
-            found = jnp.dot(picks, normed[:, low : low + tile], preferred_element_type=F32)
-            buf[pl.ds(first, n2), :, low : low + tile] = found.reshape(n2, cap, tile).astype(BF16)
+        wanted = keys[group]
+        picks = wanted[:, None, :] == lax.broadcasted_iota(
+            jnp.int32, (n2, tall, blocks * rows), 1
+        )
+        picks = jnp.where(picks, 1.0, 0.0).reshape(packed_rows, blocks * rows).astype(BF16)
+        found = jnp.dot(picks, stacked[...], preferred_element_type=F32)
+        buf[pl.ds(first, n2)] = found.reshape(n2, tall, tile).astype(BF16)
 
         def start(j):
             dst = first + (spot + 1 + j) % n2
@@ -223,7 +257,10 @@
 
     each(n1, send_group)
 
-    each(n1 - 1, lambda i: dense_wait1((plane + 1 + i) % n1))
+    for bit, following in zip(bits, bits[1:] + [None]):
+        dense_finish(bit)
+        if following is not None:
+            dense_start(following)
     each(n2 - 1, lambda i: dense_copy2((spot + 1 + i) % n2, spot).start())
 
     for i, (src, dst) in enumerate(weight_pairs):
@@ -232,6 +269,16 @@
         weight_copy(i).wait()
 
     piece = min(256, half)
+    upright = lax.broadcasted_iota(jnp.int32, (packed_rows, packed_rows), 0)
+    across = lax.broadcasted_iota(jnp.int32, (packed_rows, packed_rows), 1)
+
+    def packed_place(r):
+        return (r // cap) % n2 * tall + r // group_rows * cap + r % cap
+
+    unpack = jnp.where(packed_place(upright) == across, 1.0, 0.0).astype(BF16)
+    pack = jnp.where(packed_place(across) == upright, 1.0, 0.0).astype(BF16)
+    unpack_ref[...] = unpack
+    pack_ref[...] = pack
 
     def run_group(i):
         group = (plane - shift_of(i) + n1) % n1
@@ -245,7 +292,13 @@
                 dispatch(src, src).wait_recv()
 
         each(n2, arrive)
-        x = recv[pl.ds(first, n2)].astype(F32).reshape(n2 * cap, width).astype(BF16)
+        came = recv[pl.ds(first, n2)].astype(F32).reshape(packed_rows, tile).astype(BF16)
+        apart = jnp.dot(unpack_ref[...], came, preferred_element_type=F32)
+        for j in range(blocks):
+            xs[:, j * tile : (j + 1) * tile] = apart[
+                j * group_rows : (j + 1) * group_rows
+            ].astype(BF16)
+        x = xs[...]
         for part in range(2):
             for low in range(0, half, piece):
                 gate_pre = jnp.dot(
@@ -253,14 +306,18 @@
                 )
                 up_pre = jnp.dot(x, wus[part, :, low : low + piece], preferred_element_type=F32)
                 hid[part, :, low : low + piece] = clamped_unit(gate_pre, up_pre)
-        for low in range(0, width, tile):
-            total = jnp.zeros((n2 * cap, tile), F32)
+        for j in range(blocks):
+            total = jnp.zeros((group_rows, tile), F32)
             for part in range(2):
                 partial = jnp.dot(
-                    hid[part], wds[part, :, low : low + tile], preferred_element_type=F32
+                    hid[part],
+                    wds[part, :, j * tile : (j + 1) * tile],
+                    preferred_element_type=F32,
                 )
                 total = total + partial.astype(BF16).astype(F32)
-            outb[pl.ds(first, n2), :, low : low + tile] = total.reshape(n2, cap, tile).astype(BF16)
+            totals[j * group_rows : (j + 1) * group_rows, :] = total
+        joined = jnp.dot(pack_ref[...], totals[...].astype(BF16), preferred_element_type=F32)
+        outb[pl.ds(first, n2)] = joined.reshape(n2, tall, tile).astype(BF16)
 
         def start(j):
             dst = first + (spot + 1 + j) % n2
@@ -299,26 +356,38 @@
             jax.nn.sigmoid(dgate_ref[:, z * step : (z + 1) * step]) * branch
         )
 
-    def settle(i):
-        other = (me + 1 + i) % n
-        give_back(other, other).wait_recv()
-
-    each(n - 1, settle)
-
-    places = lax.broadcasted_iota(jnp.int32, (n, cap, rows), 1)
-    here = slots[...][:, None, :] == places
-    takes = []
-    for k in range(2):
-        mine = (routes_ref[k : k + 1, :] == expert_ids)[:, None, :]
-        take = jnp.where(here & mine, 1.0, 0.0).reshape(n * cap, rows)
-        takes.append(take.T.astype(BF16))
-    for low in range(0, width, tile):
-        back = ret[:, :, low : low + tile].astype(F32).reshape(n * cap, tile).astype(BF16)
-        total = acc[:, low : low + tile]
-        for k in range(2):
-            picked = jnp.dot(takes[k], back, preferred_element_type=F32)
-            total = total + picked * weights_ref[:, k : k + 1]
-        out_ref[:, low : low + tile] = total.astype(BF16)
+    def combine_group(i):
+        group = (plane + shift_of(i)) % n1
+        first = group * n2
+
+        def arrive(j):
+            src = first + j
+
+            @pl.when(src != me)
+            def _():
+                give_back(src, src).wait_recv()
+
+        each(n2, arrive)
+        back = ret[pl.ds(first, n2)].astype(F32).reshape(packed_rows, tile).astype(BF16)
+        lanes = lax.broadcasted_iota(jnp.int32, (rows, packed_rows), 1) + first * tall
+        wanted = jnp.concatenate(
+            [
+                jnp.where(places[:, k : k + 1] + j * cap == lanes, 1.0, 0.0).astype(BF16)
+                for k in range(2)
+                for j in range(blocks)
+            ],
+            axis=0,
+        )
+        picked = jnp.dot(wanted, back, preferred_element_type=F32)
+        for j in range(blocks):
+            total = acc[:, j * tile : (j + 1) * tile]
+            for k in range(2):
+                at = (k * blocks + j) * rows
+                total = total + picked[at : at + rows] * weights_ref[:, k : k + 1]
+            acc[:, j * tile : (j + 1) * tile] = total
+
+    each(n1, combine_group)
+    out_ref[...] = acc[...].astype(BF16)
 
     def drain(i):
         other = (me + 1 + i) % n
@@ -326,7 +395,6 @@
         give_back(other, me).wait_send()
 
     each(n - 1, drain)
-    each(n1 - 1, lambda i: dense_copy1((plane + 1 + i) % n1).wait_send())
     each(n2 - 1, lambda i: dense_copy2((spot + 1 + i) % n2, spot).wait_send())
 
 
@@ -337,7 +405,9 @@
     top_count = routes.shape[1]
     n = lax.axis_size("ep")
     capacity = (4 * rows * top_count + 3 * n - 1) // (3 * n)
-    cap = -(-capacity // 8) * 8
+    cap = capacity
+    blocks = 8 // math.gcd(cap, 8)
+    tall, tile = blocks * cap, width // blocks
     n2 = 1
     while n2 * n2 < n:
         n2 *= 2
@@ -347,15 +417,21 @@
     vmem = pl.BlockSpec(memory_space=pltpu.VMEM)
     anywhere = pl.BlockSpec(memory_space=pl.ANY)
     dma = pltpu.SemaphoreType.DMA
-    slab = pltpu.VMEM((n, cap, width), BF16)
+    slab = pltpu.VMEM((n, tall, tile), BF16)
     return pl.pallas_call(
-        functools.partial(layer_kernel, (n, n1, n2, cap)),
+        functools.partial(layer_kernel, (n, n1, n2, cap, blocks)),
         out_shape=jax.ShapeDtypeStruct((rows, width), BF16),
-        in_specs=[vmem] * 7 + [anywhere] * 3,
+        in_specs=[vmem] * 8 + [anywhere] * 3,
         out_specs=vmem,
         scratch_shapes=[
             pltpu.VMEM((rows, width), BF16),
-            pltpu.VMEM((n, rows), jnp.int32),
+            pltpu.VMEM((n1, n2, blocks * rows), jnp.int32),
+            pltpu.VMEM((blocks * rows, tile), BF16),
+            pltpu.VMEM((rows, 2), jnp.int32),
+            pltpu.VMEM((n2 * cap, width), BF16),
+            pltpu.VMEM((n2 * tall, tile), F32),
+            pltpu.VMEM((n2 * tall, n2 * tall), BF16),
+            pltpu.VMEM((n2 * tall, n2 * tall), BF16),
             slab,
             slab,
             slab,
@@ -385,6 +461,7 @@
         ),
     )(
         routes.T,
+        routes,
         route_weights,
         tokens,
         norm_gain.reshape(1, width),

time: 89.7 us -> 82 us (0.914)
  Pallas kernels: 86.2 us -> 77.1 us
  local copies, waits for them, and re-layouts: 3.29 us -> 4.7 us
    pallas_call x1, Pallas kernels: 86.2 us -> 77.1 us  [shards(): pl.pallas_call(functools.partial(layer_kernel, (n, n1, n2, cap, blocks)),...]
    unnamed x2 -> x3, local copies, waits for them, and re-layouts: 3.29 us -> 4.7 us
where the time goes in v2:
time: 82 us; the launch traced here: 81.8 us
  Pallas kernels  77.1 us (94%)
  local copies, waits for them, and re-layouts  4.7 us (6%)
    pallas_call x1, Pallas kernels, shards(): pl.pallas_call(functools.partial(layer_kernel, (n, n1, n2, cap, blocks)),...  77.1 us
    unnamed x3, local copies, waits for them, and re-layouts  4.7 us

profile of v2, /device:TPU:0, one launch (start us, length us, event | category | flops | bytes accessed | tf_op | source)
XLA Modules:
  0.0 81.8 jit_solution(1814716410163318948)
XLA Ops:
  0.0 1.4 %copy.12.weights_ref = f32[128,2]{1,0:T(8,128)} copy(f32[128,2]{0,1:T(2,128)} %param.13) | data formatting | bytes 2048 | tf_op args[3]
  1.4 1.4 %copy.11.routes_ref = s32[128,2]{1,0:T(8,128)} copy(s32[128,2]{0,1:T(2,128)} %param.12) | data formatting | bytes 2048 | tf_op args[2]
  2.8 77.1 %shard_map.100 = bf16[128,2048]{1,0:T(8,128)(2,1)} custom-call(s32[2,128]{1,0:T(2,128)} %bitcast.11, s32[128,2]{1,0:T(8,128)} %copy.11.routes_ref, f32[128,2]{1,0:T(8,128)} %copy.12.weights_ref, bf16[128,2048]{1,0:T(8,128)(2,1)} %tokens_ref.1, f32[1,2048]{1,0:T(1,128)} %bitcast.9, f32[1,2048]{1,0:T(1,128)} %bitcast.10, bf16[128,256]{1,0:T(8,128)(2,1)} %din_ref.1, ...), custom_call_target="tpu_custom_call" | custom-call | tf_op jit(solution)/shard_map/pallas_call | solution.py:421
  79.9 1.9 %copy.14 = bf16[128,2048]{1,0:T(8,128)(2,1)} copy(bf16[128,2048]{1,0:T(8,128)(2,1)} %shard_map.100) | data formatting | bytes 1048576
